TPU v7x, 512 devices: a whole 4x8x8 slice. The times are simulated.
512 devices in a mesh: sp: 64 (over z, y), fs: 4 (over x), tp: 2 (over core).
Axes of the slice: x: 4, y: 8, z: 8, core: 2. Of those that a mesh axis runs over, the one named last changes fastest.
Arguments:
- tokens: bfloat16 [16384, 2048], P(('sp', 'fs', 'tp')), may hold values from -20 to 20
- norm_gain: float32 [2048], replicated, may hold values from 0.1 to 1.9
- query_weight: bfloat16 [2048, 1024], P(None, ('fs', 'tp')), may hold values from -0.5 to 0.5
- w_key: bfloat16 [2048, 256], P(None, 'tp'), may hold values from -0.5 to 0.5
- w_value: bfloat16 [2048, 256], P(None, 'tp'), may hold values from -0.125 to 0.125
- w_input: bfloat16 [2048, 1024], P(None, ('fs', 'tp')), may hold values from -0.125 to 0.125
- w_gate: bfloat16 [2048, 1024], P(None, ('fs', 'tp')), may hold values from -0.125 to 0.125
- conv_kernel: float32 [4, 1024], P(None, ('fs', 'tp')), may hold values from -3 to 3
- w_recur: bfloat16 [16, 64, 64], P(('fs', 'tp')), may hold values from -0.75 to 0.75
- w_admit: bfloat16 [16, 64, 64], P(('fs', 'tp')), may hold values from -0.75 to 0.75
- decay_param: float32 [1024], P(('fs', 'tp')), may hold values from 4 to 17
- decay_scale: float32 [16384, 1024], P('sp', ('fs', 'tp')), may hold values from 0.5 to 229376
- init_state: float32 [1024], P(('fs', 'tp')), may hold values from -6 to 6
- diff_lambda: float32 [8], P(('fs', 'tp')), may hold values from 0.3 to 0.8
- head_gain: float32 [128], replicated, may hold values from 0.1 to 1.9
- w_out_lru: bfloat16 [1024, 2048], P(('fs', 'tp')), may hold values from -1 to 1
- w_out_attn: bfloat16 [1024, 2048], P(('fs', 'tp')), may hold values from -0.1875 to 0.1875
Outputs:
- mixed: bfloat16 [16384, 2048], P(('sp', 'fs', 'tp'))
All inputs are finite; a program needn't handle non-finite values.
Results may differ from a plain program's by a relative error of at most 0.019.
Values may be sent and summed in bfloat16 or wider, within the bound.
A program may use at most 64 MiB of HBM per device.

v0:
```python
import math

import jax
import jax.numpy as jnp
from jax import lax
from jax.sharding import Mesh
from jax.sharding import PartitionSpec as P

SP = ("sp_0", "sp_1")
SP_FS_TP = ("sp_0", "sp_1", "fs", "tp")


gate_scale = 8.0
input_eps = 1e-06
head_eps = 1e-05
far_below = -1e30


def joined_along(pieces, dim):
    dims = list(pieces.shape[1:])
    dims[dim] *= pieces.shape[0]
    return jnp.moveaxis(pieces, 0, dim).reshape(dims)


def from_everyone(value, axis):
    copies = jnp.broadcast_to(value, (lax.axis_size(axis), *value.shape))
    return lax.all_to_all(copies, axis, split_axis=0, concat_axis=0, tiled=True)


def gather_directly(value, axis, dim):
    return joined_along(from_everyone(value, axis), dim)


def passed_along(value, axis, by):
    devices = lax.axis_size(axis)
    pairs = [(i, i + by) for i in range(devices) if 0 <= i + by < devices]
    return lax.ppermute(value, axis, pairs)


def neutral_like(value, identity):
    return jax.tree.map(
        lambda part, zero: jnp.zeros_like(part) + jnp.asarray(zero, part.dtype), value, identity
    )


def prefix_by_axis(value, axes, combine, identity):
    before = start = neutral_like(value, identity)
    total = value
    for axis in reversed(axes):
        devices, here = (lax.axis_size(axis), lax.axis_index(axis))
        pieces = jax.tree.map(lambda part: lax.all_gather(part, axis), total)
        inside, total = (start, start)
        for k in range(devices):
            passed = k < here
            total = combine(total, jax.tree.map(lambda part: part[k], pieces))
            inside = jax.tree.map(lambda new, old: jnp.where(passed, new, old), total, inside)
        before = combine(inside, before)
    return before


def sent_together(arrays, axis, dim, along):
    ends, at = ([], 0)
    for a in arrays[:-1]:
        at += a.shape[along]
        ends.append(at)
    both = jnp.concatenate(arrays, axis=along)
    return tuple(jnp.split(lax.all_gather(both, axis, axis=dim, tiled=True), ends, axis=along))


def in_one_piece(arrays, axis, split_dim, concat_dim, along):
    columns = [a.reshape(*a.shape[:along], -1) for a in arrays]
    both = jnp.concatenate(columns, axis=along)
    whole, at, outs = (
        lax.all_to_all(both, axis, split_axis=split_dim, concat_axis=concat_dim, tiled=True),
        0,
        [],
    )
    for a, column in zip(arrays, columns):
        piece = whole[..., at : at + column.shape[along]]
        outs.append(piece.reshape(*piece.shape[:along], *a.shape[along:]))
        at += column.shape[along]
    return tuple(outs)


def cut_along(value, dim, devices):
    before, after = (value.shape[:dim], value.shape[dim + 1 :])
    return jnp.moveaxis(value.reshape(*before, devices, -1, *after), dim, 0)


def summed_on_arrival(value, axis, dim):
    pieces = cut_along(value, dim, lax.axis_size(axis))
    arrived = lax.all_to_all(pieces, axis, split_axis=0, concat_axis=0, tiled=True)
    return arrived.astype(jnp.float32).sum(axis=0)


def pair_combine(earlier, later):
    decay_early, state_early = earlier
    decay_late, state_late = later
    return (decay_early * decay_late, decay_late * state_early + state_late)


def fold_keys(carried, query_heads, query_pos, key_piece, value_piece, key_pos):
    total_keys = key_piece.shape[0]
    span = math.gcd(total_keys, 512)
    size_qk = query_heads.shape[-1]
    scale = size_qk ** (-0.5)

    def one_span(span_index, running):
        key_block = lax.dynamic_slice_in_dim(key_piece, span_index * span, span, 0)
        value_block = lax.dynamic_slice_in_dim(value_piece, span_index * span, span, 0)
        pos_block = lax.dynamic_slice_in_dim(key_pos, span_index * span, span, 0)

        def attend(state_now):
            peak_old, total_old, values_old = state_now
            key_maps = key_block.reshape(span, 2, size_qk)
            scores = (
                jnp.einsum(
                    "hqme,kme->hmqk", query_heads, key_maps, preferred_element_type=jnp.float32
                )
                * scale
            )
            visible = (pos_block[None, :] <= query_pos[:, None])[None, None]
            scores = jnp.where(visible, scores, far_below)
            peak_new = jnp.maximum(peak_old, jnp.max(scores, axis=-1))
            expos = jnp.where(visible, jnp.exp(scores - peak_new[..., None]), 0.0)
            fade = jnp.exp(peak_old - peak_new)
            total_new = total_old * fade + jnp.sum(expos, axis=-1)
            values_new = values_old * fade[..., None] + jnp.einsum(
                "hmqk,kv->hmqv",
                expos.astype(jnp.bfloat16),
                value_block,
                preferred_element_type=jnp.float32,
            )
            return (peak_new, total_new, values_new)

        def keep(state_now):
            return state_now

        return lax.cond(pos_block[0] <= query_pos[-1], attend, keep, running)

    return lax.fori_loop(0, total_keys // span, one_span, carried)


def empty_carry(head_count, row_count, value_size):
    return (
        jnp.full((head_count, 2, row_count), far_below, jnp.float32),
        jnp.zeros((head_count, 2, row_count), jnp.float32),
        jnp.zeros((head_count, 2, row_count, value_size), jnp.float32),
    )


def body(
    tokens,
    norm_gain,
    query_weight,
    w_key,
    w_value,
    w_input,
    w_gate,
    conv_kernel,
    w_recur,
    w_admit,
    decay_param,
    decay_scale,
    init_state,
    diff_lambda,
    head_gain,
    w_out_lru,
    w_out_attn,
):
    floats = tokens.astype(jnp.float32)
    normed = (
        floats * lax.rsqrt(jnp.mean(floats * floats, axis=1, keepdims=True) + input_eps) * norm_gain
    ).astype(jnp.bfloat16)
    weight_list = (query_weight, w_key, w_value, w_input, w_gate)

    def project_rows(piece):
        return jnp.concatenate(
            [
                jnp.dot(piece, weight, preferred_element_type=jnp.float32).astype(jnp.bfloat16)
                for weight in weight_list
            ],
            axis=1,
        )

    projected = project_rows(gather_directly(normed, ("fs", "tp"), 0))
    bounds = [0]
    for weight in weight_list:
        bounds.append(bounds[-1] + weight.shape[1])
    query = projected[:, bounds[0] : bounds[1]]
    keys_here = projected[:, bounds[1] : bounds[2]]
    values_here = projected[:, bounds[2] : bounds[3]]
    lru_in = projected[:, bounds[3] : bounds[4]]
    gate_proj = projected[:, bounds[4] : bounds[5]]
    row_count = projected.shape[0]
    channels = lru_in.shape[1]
    taps = conv_kernel.shape[0]
    earlier_rows = passed_along(lru_in[row_count - (taps - 1) :], SP, 1)
    padded = jnp.concatenate([earlier_rows, lru_in], axis=0).astype(jnp.float32)
    conv_sum = jnp.zeros((row_count, channels), jnp.float32)
    for offset in range(taps):
        conv_sum = conv_sum + conv_kernel[offset] * padded[offset : offset + row_count]
    conv_out = conv_sum.astype(jnp.bfloat16)
    grouped = conv_out.reshape(row_count, w_recur.shape[0], w_recur.shape[1])
    recur = jax.nn.sigmoid(
        jnp.einsum("tni,nij->tnj", grouped, w_recur, preferred_element_type=jnp.float32).reshape(
            row_count, channels
        )
    )
    admit = jax.nn.sigmoid(
        jnp.einsum("tni,nij->tnj", grouped, w_admit, preferred_element_type=jnp.float32).reshape(
            row_count, channels
        )
    )
    log_decay = -gate_scale * recur * jax.nn.softplus(-decay_param) * decay_scale
    decay = jnp.exp(log_decay)
    drive = jnp.sqrt(-jnp.expm1(2.0 * log_decay)) * admit * conv_out.astype(jnp.float32)
    decay_run, local_states = lax.associative_scan(pair_combine, (decay, drive), axis=0)
    identity = (jnp.ones((channels,), jnp.float32), jnp.zeros((channels,), jnp.float32))
    before_decay, before_state = prefix_by_axis(
        (decay_run[-1], local_states[-1]), SP, pair_combine, identity
    )
    entering = before_decay * init_state + before_state
    states = local_states + decay_run * entering[None, :]
    lru_out = (states * jax.nn.gelu(gate_proj.astype(jnp.float32))).astype(jnp.bfloat16)
    size_qk = query.shape[1] // 2
    value_size = values_here.shape[1]
    query_pos = lax.axis_index(SP) * row_count + jnp.arange(row_count)
    group_size = lax.axis_size("fs")
    member = lax.axis_index("fs")
    share_rows = row_count // group_size
    group_heads = gather_directly(query[None], "fs", 0)
    group_heads = group_heads.reshape(group_size, row_count, 2, size_qk)
    key_share = lax.dynamic_slice_in_dim(keys_here, member * share_rows, share_rows, 0)
    value_share = lax.dynamic_slice_in_dim(values_here, member * share_rows, share_rows, 0)
    key_piece, value_piece = sent_together((key_share, value_share), SP, 0, 1)
    collected_pointer = jnp.arange(key_piece.shape[0])
    key_pos = (
        collected_pointer // share_rows * row_count
        + member * share_rows
        + collected_pointer % share_rows
    )
    part_peak, part_total, part_values = fold_keys(
        empty_carry(group_size, row_count, value_size),
        group_heads,
        query_pos,
        key_piece,
        value_piece,
        key_pos,
    )
    part_peak, part_total, part_values = tuple(
        (
            part.astype(jnp.float32)
            for part in in_one_piece(
                (
                    part_peak.astype(jnp.bfloat16),
                    part_total.astype(jnp.bfloat16),
                    part_values.astype(jnp.bfloat16),
                ),
                "fs",
                0,
                0,
                3,
            )
        )
    )
    top_peak = jnp.max(part_peak, axis=0)
    fade = jnp.exp(part_peak - top_peak[None])
    total = jnp.sum(part_total * fade, axis=0)[None]
    heads_values = jnp.sum(part_values * fade[..., None], axis=0)[None]
    lam = diff_lambda[0]
    diff = (
        heads_values[0, 0] / total[0, 0][:, None] - lam * heads_values[0, 1] / total[0, 1][:, None]
    )
    scaled = diff * lax.rsqrt(jnp.mean(diff * diff, axis=-1, keepdims=True) + head_eps) * head_gain
    attn_out = scaled.astype(jnp.bfloat16)
    summed = summed_on_arrival(
        (
            jnp.dot(lru_out, w_out_lru, preferred_element_type=jnp.float32)
            + jnp.dot(attn_out, w_out_attn, preferred_element_type=jnp.float32)
        ).astype(jnp.bfloat16),
        ("fs", "tp"),
        0,
    )
    return summed.astype(jnp.bfloat16)


def solution(mesh):
    torus = Mesh(
        mesh.devices.reshape(8, 8, mesh.shape["fs"], mesh.shape["tp"]), ("sp_0", "sp_1", "fs", "tp")
    )
    return jax.shard_map(
        body,
        mesh=torus,
        in_specs=(
            P(SP_FS_TP, None),
            P(),
            P(None, ("fs", "tp")),
            P(None, "tp"),
            P(None, "tp"),
            P(None, ("fs", "tp")),
            P(None, ("fs", "tp")),
            P(None, ("fs", "tp")),
            P(("fs", "tp"), None, None),
            P(("fs", "tp"), None, None),
            P(("fs", "tp")),
            P(SP, ("fs", "tp")),
            P(("fs", "tp")),
            P(("fs", "tp")),
            P(),
            P(("fs", "tp"), None),
            P(("fs", "tp"), None),
        ),
        out_specs=P(SP_FS_TP, None),
        check_vma=False,
    )
```

profile of v0, /device:TPU:448, one launch (start us, length us, event | category | flops | bytes accessed | tf_op | source)
XLA Modules:
  0.0 231.8 jit_solution(10339489891016880196)
XLA Ops:
  6.5 1.2 fusion.19
  7.7 1.0 fusion.21
  8.7 1.1 broadcast_in_dim.64
  9.8 4.3 %all-to-all-start = ((bf16[8,32,2048]{2,1,0:T(8,128)(2,1)}), bf16[8,32,2048]{2,1,0:T(8,128)(2,1)S(1)}, u32[]{:S(2)}, u32[]{:S(2)}) async-start(bf16[8,32,2048]{2,1,0:T(8,128)(2,1)} %broadcast_in_dim.64), calls=%async_computation | async-start | bytes 2097152 | tf_op jit(solution)/shard_map/all_to_all | solution.py:27
  16.7 0.8 slice_bitcast_fusion.21
  17.6 12.5 %all-to-all-done = bf16[8,32,2048]{2,1,0:T(8,128)(2,1)S(1)} async-done(((bf16[8,32,2048]{2,1,0:T(8,128)(2,1)}), bf16[8,32,2048]{2,1,0:T(8,128)(2,1)S(1)}, u32[]{:S(2)}, u32[]{:S(2)}) %all-to-all-start) | async-done | bytes 1048608 | tf_op jit(solution)/shard_map/all_to_all | solution.py:27
  30.1 1.5 fusion.103
  33.1 3.5 %collective-permute-start = (bf16[3,128]{1,0:T(4,128)(2,1)S(1)}, bf16[3,128]{1,0:T(4,128)(2,1)S(1)}, u32[]{:S(2)}, u32[]{:S(2)}) collective-permute-start(bf16[3,128]{1,0:T(4,128)(2,1)S(1)} %slice.550), channel_id=1, source_target_pairs={{0,8},{8,16},{16,24},{24,32},{32,40},{40,48},{48,56},{56,64},{64,7... | collective-permute-start | bytes 2312 | tf_op jit(solution)/shard_map/ppermute | solution.py:37
  37.9 3.4 %all-to-all-start.1 = ((bf16[4,1,256,128]{2,3,1,0:T(8,128)(2,1)}), bf16[4,1,256,128]{2,3,1,0:T(8,128)(2,1)S(1)}, u32[]{:S(2)}, u32[]{:S(2)}) async-start(bf16[4,1,256,128]{2,3,1,0:T(8,128)(2,1)} %broadcast_in_dim.69), calls=%async_computation.1 | async-start | bytes 524288 | tf_op jit(solution)/shard_map/all_to_all | solution.py:27
  44.3 16.0 %all-gather = f32[8,1,128]{2,1,0:T(1,128)S(1)} all-gather(f32[1,1,128]{2,1,0:T(1,128)S(1)} %add_bitcast_fusion.1), channel_id=1, replica_groups=mesh['sp_0'=8,'sp_1'=8,'fs'=4,'tp'=2] {'sp_1'}, dimensions={0}, use_global_device_ids=true | all-gather | bytes 4608 | tf_op jit(solution)/shard_map/all_gather | solution.py:51
  60.3 13.8 %all-gather.1 = f32[8,1,128]{2,1,0:T(1,128)} all-gather(f32[1,1,128]{2,1,0:T(1,128)S(1)} %fusion.92), channel_id=1, replica_groups=mesh['sp_0'=8,'sp_1'=8,'fs'=4,'tp'=2] {'sp_0'}, dimensions={0}, use_global_device_ids=true | all-gather | bytes 4608 | tf_op jit(solution)/shard_map/all_gather | solution.py:51
  74.2 13.9 %all-gather.2 = f32[8,1,128]{2,1,0:T(1,128)S(1)} all-gather(f32[1,1,128]{2,1,0:T(1,128)S(1)} %add_bitcast_fusion), channel_id=1, replica_groups=mesh['sp_0'=8,'sp_1'=8,'fs'=4,'tp'=2] {'sp_1'}, dimensions={0}, use_global_device_ids=true | all-gather | bytes 4608 | tf_op jit(solution)/shard_map/all_gather | solution.py:51
  88.1 16.6 %all-gather.3 = f32[8,1,128]{2,1,0:T(1,128)} all-gather(f32[1,1,128]{2,1,0:T(1,128)S(1)} %fusion.84), channel_id=1, replica_groups=mesh['sp_0'=8,'sp_1'=8,'fs'=4,'tp'=2] {'sp_0'}, dimensions={0}, use_global_device_ids=true | all-gather | bytes 4608 | tf_op jit(solution)/shard_map/all_gather | solution.py:51
  104.8 7.2 %all-gather.6.cloned.1.call-done = bf16[4096,256]{1,0:T(8,128)(2,1)} async-done(((bf16[64,256]{1,0:T(8,128)(2,1)}), bf16[4096,256]{1,0:T(8,128)(2,1)}) %all-gather.6.cloned.1.call-update) | async-done | bytes 2097168 | tf_op jit(solution)/shard_map/all_gather | solution.py:67
  112.0 2.7 %fusion.99 = (bf16[4096,128]{1,0:T(8,128)(2,1)}, bf16[4096,128]{1,0:T(8,128)(2,1)S(1)}) fusion(bf16[4096,256]{1,0:T(8,128)(2,1)} %all-gather.6.cloned.1.call-done), kind=kLoop, calls=%fused_computation.268 | loop fusion | bytes 4194304 | tf_op jit(solution)/shard_map/split | solution.py:67
  114.6 1.3 copy.69
  116.0 66.8 %while.17 = (s32[]{:T(128)}, f32[4,2,256]{2,0,1:T(4,128)S(1)}, f32[4,2,256]{2,0,1:T(4,128)S(1)}, f32[4,2,256,128]{3,2,1,0:T(8,128)S(1)}, s32[4096]{0:T(1024)}, /...) while((s32[]{:T(128)}, f32[4,2,256]{2,0,1:T(4,128)S(1)}, ...), condition=%wide.region_6.7_spmd, body=%wide.region_1.6_spmd.sunk | while | flops 412749824 | bytes 16006993 | solution.py:141
  119.0 5.4 %conditional.2 = ((f32[4,2,256]{2,0,1:T(4,128)S(1)}, f32[4,2,256]{2,0,1:T(4,128)S(1)}, f32[4,2,256,128]{3,2,1,0:T(8,128)S(1)})) conditional(s32[]{:T(128)} %bitcast.358, (f32[4,2,256]{2,0,1:T(4,128)S(1)}, f32[4,2,256]{2,0,1:T(4,128)S(1)}, f32[4,2,256,128]{3,2,1,0:T(8,128)S(1)}) %tuple.78, (s32[512]{0:T(512)S(1)}, s32[256]{0:T(256)S(1)}, ...), branch_computations={%region_2.2_spmd, %region_3.5_spmd} | conditional | flops 412749824 | bytes 16002596 | solution.py:139
  119.0 0.9 constant_dynamic-slice_fusion
  120.1 0.8 fusion
  120.9 1.1 fusion.1
  122.1 2.3 fusion.5
  127.4 5.3 %conditional.2 = ((f32[4,2,256]{2,0,1:T(4,128)S(1)}, f32[4,2,256]{2,0,1:T(4,128)S(1)}, f32[4,2,256,128]{3,2,1,0:T(8,128)S(1)})) conditional(s32[]{:T(128)} %bitcast.358, (f32[4,2,256]{2,0,1:T(4,128)S(1)}, f32[4,2,256]{2,0,1:T(4,128)S(1)}, f32[4,2,256,128]{3,2,1,0:T(8,128)S(1)}) %tuple.78, (s32[512]{0:T(512)S(1)}, s32[256]{0:T(256)S(1)}, ...), branch_computations={%region_2.2_spmd, %region_3.5_spmd} | conditional | flops 412749824 | bytes 16002596 | solution.py:139
  127.4 0.9 constant_dynamic-slice_fusion
  129.3 1.1 fusion.1
  130.4 2.3 fusion.5
  135.7 5.4 %conditional.2 = ((f32[4,2,256]{2,0,1:T(4,128)S(1)}, f32[4,2,256]{2,0,1:T(4,128)S(1)}, f32[4,2,256,128]{3,2,1,0:T(8,128)S(1)})) conditional(s32[]{:T(128)} %bitcast.358, (f32[4,2,256]{2,0,1:T(4,128)S(1)}, f32[4,2,256]{2,0,1:T(4,128)S(1)}, f32[4,2,256,128]{3,2,1,0:T(8,128)S(1)}) %tuple.78, (s32[512]{0:T(512)S(1)}, s32[256]{0:T(256)S(1)}, ...), branch_computations={%region_2.2_spmd, %region_3.5_spmd} | conditional | flops 412749824 | bytes 16002596 | solution.py:139
  135.7 0.9 constant_dynamic-slice_fusion
  137.6 1.1 fusion.1
  138.8 2.3 fusion.5
  144.1 5.4 %conditional.2 = ((f32[4,2,256]{2,0,1:T(4,128)S(1)}, f32[4,2,256]{2,0,1:T(4,128)S(1)}, f32[4,2,256,128]{3,2,1,0:T(8,128)S(1)})) conditional(s32[]{:T(128)} %bitcast.358, (f32[4,2,256]{2,0,1:T(4,128)S(1)}, f32[4,2,256]{2,0,1:T(4,128)S(1)}, f32[4,2,256,128]{3,2,1,0:T(8,128)S(1)}) %tuple.78, (s32[512]{0:T(512)S(1)}, s32[256]{0:T(256)S(1)}, ...), branch_computations={%region_2.2_spmd, %region_3.5_spmd} | conditional | flops 412749824 | bytes 16002596 | solution.py:139
  144.1 0.9 constant_dynamic-slice_fusion
  145.2 0.8 fusion
  146.0 1.1 fusion.1
  147.1 2.3 fusion.5
  152.4 5.3 %conditional.2 = ((f32[4,2,256]{2,0,1:T(4,128)S(1)}, f32[4,2,256]{2,0,1:T(4,128)S(1)}, f32[4,2,256,128]{3,2,1,0:T(8,128)S(1)})) conditional(s32[]{:T(128)} %bitcast.358, (f32[4,2,256]{2,0,1:T(4,128)S(1)}, f32[4,2,256]{2,0,1:T(4,128)S(1)}, f32[4,2,256,128]{3,2,1,0:T(8,128)S(1)}) %tuple.78, (s32[512]{0:T(512)S(1)}, s32[256]{0:T(256)S(1)}, ...), branch_computations={%region_2.2_spmd, %region_3.5_spmd} | conditional | flops 412749824 | bytes 16002596 | solution.py:139
  152.4 0.9 constant_dynamic-slice_fusion
  154.3 1.1 fusion.1
  155.5 2.3 fusion.5
  160.8 5.4 %conditional.2 = ((f32[4,2,256]{2,0,1:T(4,128)S(1)}, f32[4,2,256]{2,0,1:T(4,128)S(1)}, f32[4,2,256,128]{3,2,1,0:T(8,128)S(1)})) conditional(s32[]{:T(128)} %bitcast.358, (f32[4,2,256]{2,0,1:T(4,128)S(1)}, f32[4,2,256]{2,0,1:T(4,128)S(1)}, f32[4,2,256,128]{3,2,1,0:T(8,128)S(1)}) %tuple.78, (s32[512]{0:T(512)S(1)}, s32[256]{0:T(256)S(1)}, ...), branch_computations={%region_2.2_spmd, %region_3.5_spmd} | conditional | flops 412749824 | bytes 16002596 | solution.py:139
  160.8 0.9 constant_dynamic-slice_fusion
  162.7 1.1 fusion.1
  163.8 2.3 fusion.5
  169.1 5.4 %conditional.2 = ((f32[4,2,256]{2,0,1:T(4,128)S(1)}, f32[4,2,256]{2,0,1:T(4,128)S(1)}, f32[4,2,256,128]{3,2,1,0:T(8,128)S(1)})) conditional(s32[]{:T(128)} %bitcast.358, (f32[4,2,256]{2,0,1:T(4,128)S(1)}, f32[4,2,256]{2,0,1:T(4,128)S(1)}, f32[4,2,256,128]{3,2,1,0:T(8,128)S(1)}) %tuple.78, (s32[512]{0:T(512)S(1)}, s32[256]{0:T(256)S(1)}, ...), branch_computations={%region_2.2_spmd, %region_3.5_spmd} | conditional | flops 412749824 | bytes 16002596 | solution.py:139
  169.1 0.9 constant_dynamic-slice_fusion
  171.0 1.1 fusion.1
  172.2 2.3 fusion.5
  177.5 5.3 %conditional.2 = ((f32[4,2,256]{2,0,1:T(4,128)S(1)}, f32[4,2,256]{2,0,1:T(4,128)S(1)}, f32[4,2,256,128]{3,2,1,0:T(8,128)S(1)})) conditional(s32[]{:T(128)} %bitcast.358, (f32[4,2,256]{2,0,1:T(4,128)S(1)}, f32[4,2,256]{2,0,1:T(4,128)S(1)}, f32[4,2,256,128]{3,2,1,0:T(8,128)S(1)}) %tuple.78, (s32[512]{0:T(512)S(1)}, s32[256]{0:T(256)S(1)}, ...), branch_computations={%region_2.2_spmd, %region_3.5_spmd} | conditional | flops 412749824 | bytes 16002596 | solution.py:139
  177.5 0.9 constant_dynamic-slice_fusion
  179.4 1.1 fusion.1
  180.5 2.3 fusion.5
  183.5 1.5 pad_maximum_fusion
  185.0 4.2 %all-to-all-start.2 = ((bf16[4,2,256,130]{2,1,3,0:T(2,128)(2,1)}), bf16[4,2,256,130]{2,1,3,0:T(2,128)(2,1)S(1)}, u32[]{:S(2)}, u32[]{:S(2)}) async-start(bf16[4,2,256,130]{2,1,3,0:T(2,128)(2,1)} %pad_maximum_fusion), calls=%async_computation.2 | async-start | bytes 1064960 | tf_op jit(solution)/shard_map/all_to_all | solution.py:74
  189.3 0.8 fusion.72
  190.1 3.2 %fusion.31 = f32[256,2048]{1,0:T(8,128)} fusion(bf16[128,2048]{1,0:T(8,128)(2,1)S(1)} %copy-done, bf16[256,2048]{1,0:T(8,128)(2,1)S(1)} %bitcast.364, bf16[2048,128]{1,0:T(8,128)(2,1)} %param.27, f32[256,128]{1,0:T(8,128)S(1)} %pad.128, f32[256,128]{1,0:T(8,128)S(1)} %pad.129, f32[256,128]{1,0:T(8,128)} %copy-done.5, f32[256,128]{1,0:T(8,128)S(1)} %pad.113, ...), kind=kOutput, calls=%fused_computation.46 | convolution fusion | flops 268959744 | bytes 4719104 | tf_op jit(solution)/shard_map/dot_general | solution.py:279
  193.3 4.1 %all-to-all-done.2 = bf16[4,2,256,130]{2,1,3,0:T(2,128)(2,1)S(1)} async-done(((bf16[4,2,256,130]{2,1,3,0:T(2,128)(2,1)}), bf16[4,2,256,130]{2,1,3,0:T(2,128)(2,1)S(1)}, u32[]{:S(2)}, u32[]{:S(2)}) %all-to-all-start.2) | async-done | bytes 532512 | tf_op jit(solution)/shard_map/all_to_all | solution.py:74
  197.4 1.2 slice.617
  198.6 2.0 copy.92
  200.6 1.4 multiply_reduce_fusion
  202.0 0.8 copy.91
  202.8 1.3 fusion.100
  204.2 1.6 fusion.11
  205.8 18.4 %all_to_all.20 = bf16[8,32,2048]{2,1,0:T(8,128)(2,1)S(1)} all-to-all(bf16[8,32,2048]{2,1,0:T(8,128)(2,1)S(1)} %bitcast.366), channel_id=1, replica_groups=mesh['sp_0'=8,'sp_1'=8,'fs'=4,'tp'=2] {'fs','tp'}, dimensions={0} | all-to-all | bytes 2097152 | tf_op jit(solution)/shard_map/all_to_all | solution.py:92
  224.2 0.8 reduce_sum.63
  (262 shorter events, 28.8 us)
Async XLA Ops:
  6.5 183.6 %copy-start = (bf16[128,2048]{1,0:T(8,128)(2,1)S(1)}, bf16[128,2048]{1,0:T(8,128)(2,1)}, u32[]{:S(2)}) copy-start(bf16[128,2048]{1,0:T(8,128)(2,1)} %param.36) | copy-start | bytes 1572868
  6.5 25.0 %copy-start.2 = (bf16[2048,128]{1,0:T(8,128)(2,1)S(1)}, bf16[2048,128]{1,0:T(8,128)(2,1)}, u32[]{:S(2)}) copy-start(bf16[2048,128]{1,0:T(8,128)(2,1)} %param.25) | copy-start | bytes 1572868
  6.5 26.1 %copy-start.3 = (bf16[2048,128]{1,0:T(8,128)(2,1)S(1)}, bf16[2048,128]{1,0:T(8,128)(2,1)}, u32[]{:S(2)}) copy-start(bf16[2048,128]{1,0:T(8,128)(2,1)} %param.26) | copy-start | bytes 1572868
  8.7 27.9 %copy-start.4 = (bf16[2048,128]{1,0:T(8,128)(2,1)S(1)}, bf16[2048,128]{1,0:T(8,128)(2,1)}, u32[]{:S(2)}) copy-start(bf16[2048,128]{1,0:T(8,128)(2,1)} %param.23) | copy-start | bytes 1572868
  9.8 20.2 %all-to-all-start = ((bf16[8,32,2048]{2,1,0:T(8,128)(2,1)}), bf16[8,32,2048]{2,1,0:T(8,128)(2,1)S(1)}, u32[]{:S(2)}, u32[]{:S(2)}) async-start(bf16[8,32,2048]{2,1,0:T(8,128)(2,1)} %broadcast_in_dim.64), calls=%async_computation | async-start | bytes 2097152 | tf_op jit(solution)/shard_map/all_to_all | solution.py:27
  14.1 97.8 %all-gather.6.cloned.1.call-start = ((), (), s32[]{:S(2)}) async-start(), calls=%async_computation.4 | async-start | bytes 2129920 | tf_op jit(solution)/shard_map/all_gather | solution.py:67
  30.1 11.4 %copy-start.11 = (bf16[2,64,64]{2,1,0:T(8,128)(2,1)S(1)}, bf16[2,64,64]{2,1,0:T(8,128)(2,1)}, u32[]{:S(2)}) copy-start(bf16[2,64,64]{2,1,0:T(8,128)(2,1)} %param.29) | copy-start | bytes 49156
  31.6 10.3 %copy-start.12 = (bf16[2,64,64]{2,1,0:T(8,128)(2,1)S(1)}, bf16[2,64,64]{2,1,0:T(8,128)(2,1)}, u32[]{:S(2)}) copy-start(bf16[2,64,64]{2,1,0:T(8,128)(2,1)} %param.30) | copy-start | bytes 49156
  31.6 10.6 %copy-start.6 = (f32[256,128]{1,0:T(8,128)S(1)}, f32[256,128]{1,0:T(8,128)}, u32[]{:S(2)}) copy-start(f32[256,128]{1,0:T(8,128)} %param.32) | copy-start | bytes 393220
  33.1 8.2 %collective-permute-start = (bf16[3,128]{1,0:T(4,128)(2,1)S(1)}, bf16[3,128]{1,0:T(4,128)(2,1)S(1)}, u32[]{:S(2)}, u32[]{:S(2)}) collective-permute-start(bf16[3,128]{1,0:T(4,128)(2,1)S(1)} %slice.550), channel_id=1, source_target_pairs={{0,8},{8,16},{16,24},{24,32},{32,40},{40,48},{48,56},{56,64},{64,7... | collective-permute-start | bytes 2312 | tf_op jit(solution)/shard_map/ppermute | solution.py:37
  37.9 66.8 %all-to-all-start.1 = ((bf16[4,1,256,128]{2,3,1,0:T(8,128)(2,1)}), bf16[4,1,256,128]{2,3,1,0:T(8,128)(2,1)S(1)}, u32[]{:S(2)}, u32[]{:S(2)}) async-start(bf16[4,1,256,128]{2,3,1,0:T(8,128)(2,1)} %broadcast_in_dim.69), calls=%async_computation.1 | async-start | bytes 524288 | tf_op jit(solution)/shard_map/all_to_all | solution.py:27
  44.2 71.8 %copy-start.9 = (s32[256]{0:T(256)S(1)}, s32[256]{0:T(256)}, u32[]{:S(2)}) copy-start(s32[256]{0:T(256)} %iota_add_fusion) | copy-start | bytes 3076
  44.3 60.5 %copy-start.5 = (f32[256,128]{1,0:T(8,128)}, f32[256,128]{1,0:T(8,128)S(1)}, u32[]{:S(2)}) copy-start(f32[256,128]{1,0:T(8,128)S(1)} %pad.112) | copy-start | bytes 393220
  60.3 44.4 %copy-start.7 = (f32[8,1,128]{2,1,0:T(1,128)}, f32[8,1,128]{2,1,0:T(1,128)S(1)}, u32[]{:S(2)}) copy-start(f32[8,1,128]{2,1,0:T(1,128)S(1)} %all-gather) | copy-start | bytes 12292
  88.1 16.6 %copy-start.8 = (f32[8,1,128]{2,1,0:T(1,128)}, f32[8,1,128]{2,1,0:T(1,128)S(1)}, u32[]{:S(2)}) copy-start(f32[8,1,128]{2,1,0:T(1,128)S(1)} %all-gather.2) | copy-start | bytes 12292
  185.0 12.4 %all-to-all-start.2 = ((bf16[4,2,256,130]{2,1,3,0:T(2,128)(2,1)}), bf16[4,2,256,130]{2,1,3,0:T(2,128)(2,1)S(1)}, u32[]{:S(2)}, u32[]{:S(2)}) async-start(bf16[4,2,256,130]{2,1,3,0:T(2,128)(2,1)} %pad_maximum_fusion), calls=%async_computation.2 | async-start | bytes 1064960 | tf_op jit(solution)/shard_map/all_to_all | solution.py:74
  190.1 14.0 %copy-start.10 = (f32[128]{0:T(128)S(1)}, f32[128]{0:T(128)}, u32[]{:S(2)}) copy-start(f32[128]{0:T(128)} %param.35) | copy-start | bytes 1540
  193.3 10.8 %copy-start.1 = (f32[256,2048]{1,0:T(8,128)S(1)}, f32[256,2048]{1,0:T(8,128)}, u32[]{:S(2)}) copy-start(f32[256,2048]{1,0:T(8,128)} %fusion.31) | copy-start | bytes 6291460
Sparse Core Ops, SparseCore 0:
  32.8 79.1 all-gather.5
where the time goes:
time: 233 us; the launch traced here: 232 us
  blocking collectives  78.8 us (34%)
  local copies, waits for them, and re-layouts  34.8 us (15%)
  matrix products  32.8 us (14%)
  waiting for transfers between devices  23.8 us (10%)
  other arithmetic  21.3 us (9%)
  starting transfers between devices  15.5 us (7%)
  between operations  15.1 us (6%)
  loops' own time  9.79 us (4%)
    all_gather x4, blocking collectives, prefix_by_axis(): pieces = jax.tree.map(lambda part: lax.all_gather(part, axis), total)  60.4 us
    all_to_all x1, blocking collectives, summed_on_arrival(): lax.all_to_all(pieces, axis, split_axis=0, concat_axis=0, tiled=True)  18.4 us
    dot_general x8, matrix products, attend(): jnp.einsum('hmqk,kv->hmqv', expos.astype(jnp.bfloat16), value_block, pref...  18.3 us
    all_to_all x2, waiting for transfers between devices, from_everyone(): return lax.all_to_all(copies, axis, split_axis=0, concat_axis=0, tiled=True)  12.5 us
    another operation x1, loops' own time, fold_keys(): return lax.fori_loop(0, total_keys // span, one_span, carried)  9.24 us
    convert_element_type x8, other arithmetic, attend(): expos.astype(jnp.bfloat16)  8.79 us
    slice x16, local copies, waits for them, and re-layouts, one_span(): return lax.cond(pos_block[0] <= query_pos[-1], attend, keep, running)  8.7 us
    all_to_all x2, starting transfers between devices, from_everyone(): return lax.all_to_all(copies, axis, split_axis=0, concat_axis=0, tiled=True)  7.7 us
  transfers between devices with their start and end apart: 5, of which 3 were waited for; matrix products, arithmetic and copies ran while one was open for 5% of the time, Pallas kernels for 0%

commit v1 on v0

v1 whole, which is shorter than its diff:
```python
import functools
import math

import jax
import jax.numpy as jnp
from jax import lax
from jax.experimental import pallas as pl
from jax.experimental.pallas import tpu as pltpu
from jax.sharding import Mesh
from jax.sharding import PartitionSpec as P

SP = ("sp_0", "sp_1")
SP_FS_TP = ("sp_0", "sp_1", "fs", "tp")
MESH = pl.DeviceIdType.MESH
BF = jnp.bfloat16
F32 = jnp.float32

gate_scale = 8.0
input_eps = 1e-06
head_eps = 1e-05
far_below = -1e30


def remote(src, dst, send, recv, where):
    return pltpu.make_async_remote_copy(
        src_ref=src, dst_ref=dst, send_sem=send, recv_sem=recv,
        device_id=where, device_id_type=MESH,
    )


def greet(peers):
    barrier = pltpu.get_barrier_semaphore()
    for peer in peers:
        pl.semaphore_signal(barrier, inc=1, device_id=peer, device_id_type=MESH)
    pl.semaphore_wait(barrier, len(peers))


def project_kernel(q_scale, tok, gain, wq, wk, wv, wi, wg, q_out, kv_out, lru_out, gate_out,
                   xbuf, nbuf, wbuf, wsem, tsem, ssem, rsem):
    x, c = lax.axis_index("fs"), lax.axis_index("tp")
    left, right, opp = lax.rem(x + 3, 4), lax.rem(x + 1, 4), lax.rem(x + 2, 4)
    rows = tok.shape[0]
    half = rows // 2
    me = 2 * x + c
    weights = [
        pltpu.make_async_copy(w, wbuf.at[:, pl.ds(128 * i, 128)], wsem.at[i])
        for i, w in enumerate((wq, wk, wv, wi, wg))
    ]
    mine = pltpu.make_async_copy(tok, xbuf.at[me], tsem)
    mine.start()
    for copy in weights:
        copy.start()
    greet([{"tp": 1 - c}, {"fs": left}, {"fs": right}])
    mine.wait()

    def piece(chip, core, part):
        ref = xbuf.at[2 * chip + core]
        if part is None:
            return ref
        return ref.at[pl.ds(part * half, half)]

    started = []

    def send(k, chip, core, part, where):
        ref = piece(chip, core, part)
        copy = remote(ref, ref, ssem.at[k], rsem.at[k], where)
        copy.start()
        started.append(copy)

    def arrive(k, chip, core, part):
        ref = piece(chip, core, part)
        remote(ref, ref, ssem.at[k], rsem.at[k], {"tp": 1 - c}).wait_recv()

    def norm(chip, core):
        slot = 2 * chip + core
        t = xbuf[slot].astype(F32)
        ms = jnp.mean(t * t, axis=1, keepdims=True)
        nbuf[pl.ds(pl.multiple_of(slot * rows, rows), rows), :] = (
            t * lax.rsqrt(ms + input_eps) * gain[...]
        ).astype(BF)

    sib = {"tp": 1 - c}
    to_right, to_left = {"fs": right}, {"fs": left}
    send(1, x, c, 0, to_right)
    send(3, x, c, 1, to_left)
    send(2, x, c, 1, to_right)
    send(4, x, c, 0, to_left)
    send(0, x, c, None, sib)
    norm(x, c)
    arrive(0, x, 1 - c, None)
    norm(x, 1 - c)
    arrive(1, left, c, 0)
    send(5, left, c, 0, to_right)
    send(7, left, c, 0, sib)
    arrive(3, right, c, 1)
    send(6, right, c, 1, to_left)
    send(9, right, c, 1, sib)
    arrive(2, left, c, 1)
    send(8, left, c, 1, sib)
    arrive(4, right, c, 0)
    send(10, right, c, 0, sib)
    norm(left, c)
    norm(right, c)
    arrive(7, left, 1 - c, 0)
    arrive(8, left, 1 - c, 1)
    norm(left, 1 - c)
    arrive(9, right, 1 - c, 1)
    arrive(10, right, 1 - c, 0)
    norm(right, 1 - c)
    arrive(5, opp, c, 0)
    send(11, opp, c, 0, sib)
    arrive(6, opp, c, 1)
    send(12, opp, c, 1, sib)
    norm(opp, c)
    for copy in weights:
        copy.wait()
    arrive(11, opp, 1 - c, 0)
    arrive(12, opp, 1 - c, 1)
    norm(opp, 1 - c)
    both = jnp.dot(nbuf[...], wbuf[...], preferred_element_type=F32)
    q_out[...] = (both[:, 0:128] * q_scale).astype(BF)
    kv_out[...] = both[:, 128:384].astype(BF)
    lru_out[...] = both[:, 384:512].astype(BF)
    gate_out[...] = both[:, 512:640].astype(BF)
    for copy in started:
        copy.wait_send()


def project_call(tokens, gain, wq, wk, wv, wi, wg):
    rows, d = tokens.shape
    whole = rows * 8
    vm = pl.BlockSpec(memory_space=pltpu.VMEM)
    hb = pl.BlockSpec(memory_space=pl.ANY)
    size_qk = wq.shape[1] // 2
    q_scale = size_qk ** (-0.5) * math.log2(math.e)
    return pl.pallas_call(
        functools.partial(project_kernel, q_scale),
        out_shape=[
            jax.ShapeDtypeStruct((whole, 128), BF),
            jax.ShapeDtypeStruct((whole, 256), BF),
            jax.ShapeDtypeStruct((whole, 128), BF),
            jax.ShapeDtypeStruct((whole, 128), BF),
        ],
        in_specs=[hb, vm] + [hb] * 5,
        out_specs=[vm] * 4,
        scratch_shapes=[
            pltpu.VMEM((8, rows, d), BF),
            pltpu.VMEM((whole, d), BF),
            pltpu.VMEM((d, 640), BF),
            pltpu.SemaphoreType.DMA((5,)),
            pltpu.SemaphoreType.DMA,
            pltpu.SemaphoreType.DMA((13,)),
            pltpu.SemaphoreType.DMA((13,)),
        ],
        compiler_params=pltpu.CompilerParams(collective_id=0, has_side_effects=True),
        name="project",
    )(tokens, gain.reshape(1, d), wq, wk, wv, wi, wg)


def scan_rows(a, b, rows):
    row = lax.broadcasted_iota(jnp.int32, a.shape, 0)
    d = 1
    while d < rows:
        a_early = jnp.where(row >= d, pltpu.roll(a, d, axis=0), 1.0)
        b_early = jnp.where(row >= d, pltpu.roll(b, d, axis=0), 0.0)
        b = a * b_early + b
        a = a * a_early
        d *= 2
    return a, b


def log1p_small(u):
    s = u / (2.0 + u)
    s2 = s * s
    total = jnp.full_like(s, 1.0 / 15.0)
    for k in (13, 11, 9, 7, 5, 3, 1):
        total = total * s2 + 1.0 / k
    return 2.0 * s * total


def minus_expm1(v):
    series = jnp.full_like(v, 1.0 / 11.0)
    total = 1.0 + v * series
    for k in (10, 9, 8, 7, 6, 5, 4, 3, 2):
        total = 1.0 + v * total * (1.0 / k)
    return jnp.where(v > -0.5, -v * total, 1.0 - jnp.exp(v))


def gelu(v):
    return 0.5 * v * (1.0 + jnp.tanh(math.sqrt(2.0 / math.pi) * (v + 0.044715 * v * v * v)))


def fold_pairs(buf, here, n):
    a_in = jnp.ones((1, 128), F32)
    b_in = jnp.zeros((1, 128), F32)
    a_all, b_all = a_in, b_in
    for k in range(n):
        a, b = buf[k, 0:1, :], buf[k, 1:2, :]
        a_all, b_all = a_all * a, a * b_all + b
        past = k < here
        a_in, b_in = jnp.where(past, a_all, a_in), jnp.where(past, b_all, b_in)
    return a_in, b_in, a_all, b_all


def mix_kernel(q_ref, kv_ref, lru_in, gate, taps, w_recur, w_admit, param, scale, init,
               o_ref, lse_ref, lru_out,
               kva, kvb, qbuf, qp, m_s, l_s, acc, bias_s, halo, pad, wgate, run_a, run_b, ab_y, ab_z, ab_me, lse_s,
               q_ss, q_rs, p_ss, p_rs, r_ss, r_rs, h_ss, h_rs, ab_ss, ab_rs):
    z, y = lax.axis_index("sp_0"), lax.axis_index("sp_1")
    x, c = lax.axis_index("fs"), lax.axis_index("tp")
    left, right, opp = lax.rem(x + 3, 4), lax.rem(x + 1, 4), lax.rem(x + 2, 4)
    n = 8

    def wrap(v):
        return lax.rem(v + 2 * n, n)

    sp = z * n + y
    after, before = lax.rem(sp + 1, 64), lax.rem(sp + 63, 64)
    nxt = {"sp_0": after // n, "sp_1": lax.rem(after, n)}
    prev = {"sp_0": before // n, "sp_1": lax.rem(before, n)}
    greet(
        [{"sp_1": wrap(y + d)} for d in range(1, n)]
        + [{"sp_0": wrap(z + d)} for d in range(1, n)]
        + [{"fs": left}, {"fs": right}, nxt, prev]
    )
    started = []

    def go(src, dst, ss, rs, where):
        copy = remote(src, dst, ss, rs, where)
        copy.start()
        started.append(copy)

    def took(dst, ss, rs, where):
        remote(dst, dst, ss, rs, where).wait_recv()

    def part(ref, i, at, size):
        return ref.at[i, pl.ds(pl.multiple_of(at, 32), size), :]

    base = x * 64
    src_a = kv_ref.at[pl.ds(pl.multiple_of(base, 32), 32), :]
    src_b = kv_ref.at[pl.ds(pl.multiple_of(base + 32, 32), 32), :]
    for d in (1, 7, 2, 6, 3, 5, 4):
        go(src_a, part(kva, z, y * 32, 32), p_ss.at[0, d], p_rs.at[0, d], {"sp_1": wrap(y + d)})
        go(src_b, part(kvb, y, z * 32, 32), p_ss.at[1, d], p_rs.at[1, d], {"sp_0": wrap(z + d)})
    rows = q_ref.shape[0]
    half = rows // 2

    def q_src(h):
        return q_ref.at[pl.ds(h * half, half), :]

    def q_at(chip, h):
        return qbuf.at[chip, pl.ds(h * half, half), :]

    to_right, to_left = {"fs": right}, {"fs": left}
    go(q_src(0), q_at(x, 0), q_ss.at[0], q_rs.at[0], to_right)
    go(q_src(1), q_at(x, 1), q_ss.at[1], q_rs.at[1], to_left)
    go(q_src(1), q_at(x, 1), q_ss.at[2], q_rs.at[2], to_right)
    go(q_src(0), q_at(x, 0), q_ss.at[3], q_rs.at[3], to_left)
    go(lru_in.at[pl.ds(rows - 16, 16), :], halo, h_ss, h_rs, nxt)

    kva[z, pl.ds(pl.multiple_of(y * 32, 32), 32), :] = kv_ref[pl.ds(pl.multiple_of(base, 32), 32), :]
    kvb[y, pl.ds(pl.multiple_of(z * 32, 32), 32), :] = kv_ref[pl.ds(pl.multiple_of(base + 32, 32), 32), :]

    row = lax.broadcasted_iota(jnp.int32, (rows, 256), 0)
    lane = lax.broadcasted_iota(jnp.int32, (rows, 256), 1)
    block, inner = lane // 32, lax.rem(lane, 32)
    q_pos = sp * rows + row
    key_a = (z * n + block) * rows + base + inner
    key_b = (block * n + y) * rows + base + 32 + inner
    bias_s[0] = jnp.where(key_a <= q_pos, 0.0, far_below)
    bias_s[1] = jnp.where(key_b <= q_pos, 0.0, far_below)

    first_lanes = lax.broadcasted_iota(jnp.int32, (rows, 128), 1) < 64

    def ready_q(chip, value):
        v = value.astype(F32)
        qp[2 * chip] = jnp.where(first_lanes, v, 0.0).astype(BF)
        qp[2 * chip + 1] = jnp.where(first_lanes, 0.0, v).astype(BF)

    ready_q(x, q_ref[...])
    took(q_at(left, 0), q_ss.at[0], q_rs.at[0], to_left)
    go(q_at(left, 0), q_at(left, 0), q_ss.at[4], q_rs.at[4], to_right)
    took(q_at(right, 1), q_ss.at[1], q_rs.at[1], to_right)
    go(q_at(right, 1), q_at(right, 1), q_ss.at[5], q_rs.at[5], to_left)

    def ring(which, buf, axis, me):
        up, down = {axis: wrap(me + 1)}, {axis: wrap(me - 1)}

        def half_of(i, h):
            return part(buf, i, h * 128, 128)

        def hop(s, h, direction):
            origin = wrap(me - (s - 1)) if direction == 0 else wrap(me + (s - 1))
            k = (which, direction, s - 1, h)
            go(half_of(origin, h), half_of(origin, h), r_ss.at[k], r_rs.at[k], up if direction == 0 else down)

        def land(s, h, direction):
            origin = wrap(me - s) if direction == 0 else wrap(me + s)
            k = (which, direction, s - 1, h)
            took(half_of(origin, h), r_ss.at[k], r_rs.at[k], down if direction == 0 else up)

        return hop, land

    hop_a, land_a = ring(0, kva, "sp_0", z)
    hop_b, land_b = ring(1, kvb, "sp_1", y)
    for d in range(1, n):
        took(part(kva, z, wrap(y - d) * 32, 32), p_ss.at[0, d], p_rs.at[0, d], {"sp_1": wrap(y - d)})
        took(part(kvb, y, wrap(z - d) * 32, 32), p_ss.at[1, d], p_rs.at[1, d], {"sp_0": wrap(z - d)})
    for h in (0, 1):
        for direction in (0, 1):
            hop_a(1, h, direction)
            hop_b(1, h, direction)

    took(halo, h_ss, h_rs, prev)
    pad[0:8, :] = jnp.where(sp > 0, halo[8:16, :].astype(F32), 0.0)
    pad[8:8 + rows, :] = lru_in[...].astype(F32)
    conv = jnp.zeros((rows, 128), F32)
    for j in range(4):
        conv = conv + taps[j:j + 1, :] * pad[5 + j:5 + j + rows, :]
    conv_bf = conv.astype(BF)
    wgate[...] = jnp.zeros_like(wgate)
    for i, w in enumerate((w_recur, w_admit)):
        zero = jnp.zeros((64, 64), F32)
        wgate[0:64, 128 * i:128 * i + 128] = jnp.concatenate([w[0].astype(F32), zero], axis=1).astype(BF)
        wgate[64:128, 128 * i:128 * i + 128] = jnp.concatenate([zero, w[1].astype(F32)], axis=1).astype(BF)
    gates = jnp.dot(conv_bf, wgate[...], preferred_element_type=F32)
    gates = 1.0 / (1.0 + jnp.exp(-gates))
    recur, admit = gates[:, :128], gates[:, 128:]
    p = param[...]
    soft = jnp.maximum(-p, 0.0) + log1p_small(jnp.exp(-jnp.abs(p)))
    log_decay = -gate_scale * recur * soft * scale[...]
    decay = jnp.exp(log_decay)
    drive = jnp.sqrt(minus_expm1(2.0 * log_decay)) * admit * conv_bf.astype(F32)
    a, b = scan_rows(decay, drive, rows)
    run_a[...] = a
    run_b[...] = b
    ab_me[0, 0:1, :] = run_a[rows - 1:rows, :]
    ab_me[0, 1:2, :] = run_b[rows - 1:rows, :]
    for d in range(1, n):
        go(ab_me.at[0], ab_y.at[y], ab_ss.at[0, d], ab_rs.at[0, d], {"sp_1": wrap(y + d)})

    took(q_at(left, 1), q_ss.at[2], q_rs.at[2], to_left)
    ready_q(left, qbuf[left])
    took(q_at(right, 0), q_ss.at[3], q_rs.at[3], to_right)
    ready_q(right, qbuf[right])
    took(q_at(opp, 0), q_ss.at[4], q_rs.at[4], to_left)
    took(q_at(opp, 1), q_ss.at[5], q_rs.at[5], to_right)
    ready_q(opp, qbuf[opp])

    nt = (((1,), (1,)), ((), ()))

    def attend(first, ia, ib, lim_a=None, lim_b=None):
        lane1 = lax.broadcasted_iota(jnp.int32, (1, 256), 1)
        if not first:
            row_a = jnp.where(lane1 < lim_a, 0.0, far_below)
            row_b = jnp.where(lane1 < lim_b, 0.0, far_below)

        def one(hm, carry):
            q = qp[hm]
            sa = lax.dot_general(q, kva[ia, :, 0:128], nt, preferred_element_type=F32)
            sb = lax.dot_general(q, kvb[ib, :, 0:128], nt, preferred_element_type=F32)
            if first:
                sa, sb = sa + bias_s[0], sb + bias_s[1]
            else:
                sa, sb = sa + row_a, sb + row_b
            parts = [sa[:, :128], sa[:, 128:], sb[:, :128], sb[:, 128:]]
            top = jnp.maximum(jnp.maximum(parts[0], parts[1]), jnp.maximum(parts[2], parts[3]))
            top = jnp.broadcast_to(jnp.max(top, axis=1, keepdims=True), (rows, 128))
            if first:
                m_new = top
            else:
                m_old = m_s[hm]
                m_new = jnp.maximum(m_old, top)
                fade = jnp.exp2(m_old - m_new)
            expos = [jnp.exp2(v - m_new) for v in parts]
            line = (expos[0] + expos[1]) + (expos[2] + expos[3])
            pa = jnp.concatenate([expos[0].astype(BF), expos[1].astype(BF)], axis=1)
            pb = jnp.concatenate([expos[2].astype(BF), expos[3].astype(BF)], axis=1)
            new = jnp.dot(pa, kva[ia, :, 128:256], preferred_element_type=F32)
            new = new + jnp.dot(pb, kvb[ib, :, 128:256], preferred_element_type=F32)
            m_s[hm] = m_new
            if first:
                l_s[hm] = line
                acc[hm] = new
            else:
                l_s[hm] = l_s[hm] * fade + line
                acc[hm] = acc[hm] * fade + new
            return carry

        lax.fori_loop(0, 8, one, 0)

    def pair(step):
        za, yb = wrap(z + step), wrap(y + step)
        lim_a = jnp.where(za < z, 256, 0)
        lim_b = (z + jnp.where(yb < y, 1, 0)) * 32

        @pl.when(jnp.logical_or(za < z, lim_b > 0))
        def _():
            attend(False, za, yb, lim_a, lim_b)

    attend(True, z, y)
    for s in (1, 2, 3):
        for h in (0, 1):
            for direction in (0, 1):
                land_a(s, h, direction)
                land_b(s, h, direction)
                if s < 3 or h == direction:
                    hop_a(s + 1, h, direction)
                    hop_b(s + 1, h, direction)
        pair(-s)
        pair(s)
        if s == 1:
            for d in range(1, n):
                took(ab_y.at[wrap(y - d)], ab_ss.at[0, d], ab_rs.at[0, d], {"sp_1": wrap(y - d)})
            ab_y[y] = ab_me[0]
            a_in, b_in, a_all, b_all = fold_pairs(ab_y, y, n)
            ab_me[1, 0:1, :] = a_all
            ab_me[1, 1:2, :] = b_all
            ab_me[2, 0:1, :] = a_in
            ab_me[2, 1:2, :] = b_in
            for d in range(1, n):
                go(ab_me.at[1], ab_z.at[z], ab_ss.at[1, d], ab_rs.at[1, d], {"sp_0": wrap(z + d)})
        if s == 3:
            for d in range(1, n):
                took(ab_z.at[wrap(z - d)], ab_ss.at[1, d], ab_rs.at[1, d], {"sp_0": wrap(z - d)})
            ab_z[z] = ab_me[1]
            a_out, b_out, _, _ = fold_pairs(ab_z, z, n)
            a_in, b_in = ab_me[2, 0:1, :], ab_me[2, 1:2, :]
            a_in, b_in = a_out * a_in, a_in * b_out + b_in
            entering = a_in * init[...] + b_in
            states = run_b[...] + run_a[...] * entering
            lru_out[...] = (states * gelu(gate[...].astype(F32))).astype(BF)
    for direction in (0, 1):
        land_a(4, direction, direction)
        land_b(4, direction, direction)
    pair(4)

    spot = lax.broadcasted_iota(jnp.int32, (rows, 128), 1)

    lse_s[...] = jnp.zeros_like(lse_s)

    def close(hm, carry):
        total = jnp.sum(l_s[hm], axis=1, keepdims=True)
        o_ref[hm] = (acc[hm] / total).astype(BF)
        lse = m_s[hm] + jnp.log(total) * math.log2(math.e)
        lse_s[...] = jnp.where(spot == hm, lse, lse_s[...])
        return carry

    lax.fori_loop(0, 8, close, 0)
    lse_ref[...] = jnp.transpose(lse_s[...])[0:8, :]
    for copy in started:
        copy.wait_send()


def mix_call(q, kv, lru_in, gate, taps, w_recur, w_admit, param, scale, init):
    rows = q.shape[0]
    vm = pl.BlockSpec(memory_space=pltpu.VMEM)
    dma = pltpu.SemaphoreType.DMA
    return pl.pallas_call(
        mix_kernel,
        out_shape=[
            jax.ShapeDtypeStruct((8, rows, 128), BF),
            jax.ShapeDtypeStruct((8, rows), F32),
            jax.ShapeDtypeStruct((rows, 128), BF),
        ],
        in_specs=[vm] * 10,
        out_specs=[vm] * 3,
        scratch_shapes=[
            pltpu.VMEM((8, 256, 256), BF),
            pltpu.VMEM((8, 256, 256), BF),
            pltpu.VMEM((4, rows, 128), BF),
            pltpu.VMEM((8, rows, 128), BF),
            pltpu.VMEM((8, rows, 128), F32),
            pltpu.VMEM((8, rows, 128), F32),
            pltpu.VMEM((8, rows, 128), F32),
            pltpu.VMEM((2, rows, 256), F32),
            pltpu.VMEM((16, 128), BF),
            pltpu.VMEM((rows + 8, 128), F32),
            pltpu.VMEM((128, 256), BF),
            pltpu.VMEM((rows, 128), F32),
            pltpu.VMEM((rows, 128), F32),
            pltpu.VMEM((8, 8, 128), F32),
            pltpu.VMEM((8, 8, 128), F32),
            pltpu.VMEM((3, 8, 128), F32),
            pltpu.VMEM((rows, 128), F32),
            dma((6,)), dma((6,)),
            dma((2, 8)), dma((2, 8)),
            dma((2, 2, 4, 2)), dma((2, 2, 4, 2)),
            dma, dma,
            dma((2, 8)), dma((2, 8)),
        ],
        compiler_params=pltpu.CompilerParams(collective_id=1, has_side_effects=True),
        name="mix",
    )(q, kv, lru_in, gate, taps, w_recur, w_admit, param.reshape(1, 128), scale, init.reshape(1, 128))


def output_kernel(o_ref, lse_ref, lru, lam, gain, w_lru, w_attn, out_ref,
                  got, relay, lses, lhs, wbuf, pbuf, sib_in, sbuf, r2, fin,
                  wsem, c_ss, c_rs, s_ss, s_rs):
    x, c = lax.axis_index("fs"), lax.axis_index("tp")
    left, right, opp = lax.rem(x + 3, 4), lax.rem(x + 1, 4), lax.rem(x + 2, 4)
    to_right, to_left, to_opp, sib = {"fs": right}, {"fs": left}, {"fs": opp}, {"tp": 1 - c}
    weights = [
        pltpu.make_async_copy(w_lru, wbuf.at[pl.ds(0, 128), :], wsem.at[0]),
        pltpu.make_async_copy(w_attn, wbuf.at[pl.ds(128, 128), :], wsem.at[1]),
    ]
    for copy in weights:
        copy.start()
    greet([sib, to_left, to_right, to_opp])
    started = []

    def go(src, dst, ss, rs, where):
        copy = remote(src, dst, ss, rs, where)
        copy.start()
        started.append(copy)

    def took(dst, ss, rs, where):
        remote(dst, dst, ss, rs, where).wait_recv()

    go(lse_ref, lses.at[2], c_ss.at[0], c_rs.at[0], to_opp)
    go(lse_ref, lses.at[0], c_ss.at[1], c_rs.at[1], to_right)
    go(lse_ref, lses.at[1], c_ss.at[2], c_rs.at[2], to_left)
    go(o_ref.at[2 * opp], relay.at[0], c_ss.at[3], c_rs.at[3], to_right)
    go(o_ref.at[2 * opp + 1], relay.at[1], c_ss.at[4], c_rs.at[4], to_left)
    go(o_ref.at[pl.ds(2 * right, 2)], got.at[0], c_ss.at[5], c_rs.at[5], to_right)
    go(o_ref.at[pl.ds(2 * left, 2)], got.at[1], c_ss.at[6], c_rs.at[6], to_left)
    took(relay.at[0], c_ss.at[3], c_rs.at[3], to_left)
    go(relay.at[0], got.at[2, 0], c_ss.at[7], c_rs.at[7], to_right)
    took(relay.at[1], c_ss.at[4], c_rs.at[4], to_right)
    go(relay.at[1], got.at[2, 1], c_ss.at[8], c_rs.at[8], to_left)
    rows = lru.shape[0]
    lhs[:, 0:128] = lru[...]
    took(lses.at[2], c_ss.at[0], c_rs.at[0], to_opp)
    took(lses.at[0], c_ss.at[1], c_rs.at[1], to_left)
    took(lses.at[1], c_ss.at[2], c_rs.at[2], to_right)

    def column(line):
        return jnp.transpose(jnp.broadcast_to(line, (128, rows)))

    heads = []
    shares = []
    for m in (0, 1):
        lines = [lse_ref[pl.ds(2 * x + m, 1), :]] + [lses[i, pl.ds(2 * x + m, 1), :] for i in range(3)]
        top = functools.reduce(jnp.maximum, lines)
        powers = [jnp.exp2(v - top) for v in lines]
        total = functools.reduce(jnp.add, powers)
        shares.append([column(v / total) for v in powers])
    took(got.at[0], c_ss.at[5], c_rs.at[5], to_left)
    took(got.at[1], c_ss.at[6], c_rs.at[6], to_right)
    took(got.at[2, 0], c_ss.at[7], c_rs.at[7], to_left)
    took(got.at[2, 1], c_ss.at[8], c_rs.at[8], to_right)
    for m in (0, 1):
        value = shares[m][0] * o_ref[2 * x + m].astype(F32)
        for i in range(3):
            value = value + shares[m][1 + i] * got[i, m].astype(F32)
        heads.append(value)
    diff = heads[0] - lam[...] * heads[1]
    ms = jnp.mean(diff * diff, axis=1, keepdims=True)
    lhs[:, 128:256] = (diff * lax.rsqrt(ms + head_eps) * gain[...]).astype(BF)
    for copy in weights:
        copy.wait()

    def make(chip, k):
        at = pl.multiple_of(chip * 64, 64)
        value = jnp.dot(lhs[pl.ds(at, 64), :], wbuf[...], preferred_element_type=F32)
        pbuf[k] = value.astype(BF).reshape(2, 32, value.shape[1])
        go(pbuf.at[k, 1 - c], sib_in.at[k], s_ss.at[k], s_rs.at[k], sib)

    def both(k):
        took(sib_in.at[k], s_ss.at[k], s_rs.at[k], sib)
        return pbuf[k, c].astype(F32) + sib_in[k].astype(F32)

    make(opp, 0)
    make(right, 1)
    make(left, 2)
    sbuf[0] = both(0).astype(BF)
    go(sbuf.at[0, pl.ds(0, 16), :], r2.at[0], s_ss.at[4], s_rs.at[4], to_right)
    go(sbuf.at[0, pl.ds(16, 16), :], r2.at[1], s_ss.at[5], s_rs.at[5], to_left)
    make(x, 3)
    sum_right, sum_left = both(1), both(2)
    sbuf[1, 16:32] = sum_right[16:32].astype(BF)
    sbuf[2, 0:16] = sum_left[0:16].astype(BF)
    took(r2.at[0], s_ss.at[4], s_rs.at[4], to_left)
    sbuf[1, 0:16] = (sum_right[0:16] + r2[0].astype(F32)).astype(BF)
    go(sbuf.at[1], fin.at[0], s_ss.at[6], s_rs.at[6], to_right)
    took(r2.at[1], s_ss.at[5], s_rs.at[5], to_right)
    sbuf[2, 16:32] = (sum_left[16:32] + r2[1].astype(F32)).astype(BF)
    go(sbuf.at[2], fin.at[1], s_ss.at[7], s_rs.at[7], to_left)
    own = both(3)
    took(fin.at[0], s_ss.at[6], s_rs.at[6], to_left)
    took(fin.at[1], s_ss.at[7], s_rs.at[7], to_right)
    out_ref[...] = (own + fin[0].astype(F32) + fin[1].astype(F32)).astype(BF)
    for copy in started:
        copy.wait_send()


def output_call(o, lse, lru, lam, gain, w_lru, w_attn):
    rows, d = lru.shape[0], w_lru.shape[1]
    vm = pl.BlockSpec(memory_space=pltpu.VMEM)
    hb = pl.BlockSpec(memory_space=pl.ANY)
    dma = pltpu.SemaphoreType.DMA
    return pl.pallas_call(
        output_kernel,
        out_shape=jax.ShapeDtypeStruct((rows // 8, d), BF),
        in_specs=[vm] * 5 + [hb] * 2,
        out_specs=vm,
        scratch_shapes=[
            pltpu.VMEM((3, 2, rows, 128), BF),
            pltpu.VMEM((2, rows, 128), BF),
            pltpu.VMEM((3, 8, rows), F32),
            pltpu.VMEM((rows, 256), BF),
            pltpu.VMEM((256, d), BF),
            pltpu.VMEM((4, 2, 32, d), BF),
            pltpu.VMEM((4, 32, d), BF),
            pltpu.VMEM((3, 32, d), BF),
            pltpu.VMEM((2, 16, d), BF),
            pltpu.VMEM((2, 32, d), BF),
            dma((2,)),
            dma((9,)), dma((9,)),
            dma((8,)), dma((8,)),
        ],
        compiler_params=pltpu.CompilerParams(collective_id=2, has_side_effects=True),
        name="output",
    )(o, lse, lru, jnp.broadcast_to(lam.reshape(1, 1), (1, 128)), gain.reshape(1, 128), w_lru, w_attn)


def body(tokens, norm_gain, query_weight, w_key, w_value, w_input, w_gate, conv_kernel, w_recur, w_admit,
         decay_param, decay_scale, init_state, diff_lambda, head_gain, w_out_lru, w_out_attn):
    q, kv, lru_in, gate = project_call(tokens, norm_gain, query_weight, w_key, w_value, w_input, w_gate)
    o, lse, lru = mix_call(
        q, kv, lru_in, gate, conv_kernel, w_recur, w_admit, decay_param, decay_scale, init_state
    )
    return output_call(o, lse, lru, diff_lambda, head_gain, w_out_lru, w_out_attn)


def solution(mesh):
    torus = Mesh(
        mesh.devices.reshape(8, 8, mesh.shape["fs"], mesh.shape["tp"]), ("sp_0", "sp_1", "fs", "tp")
    )
    return jax.shard_map(
        body,
        mesh=torus,
        in_specs=(
            P(SP_FS_TP, None),
            P(),
            P(None, ("fs", "tp")),
            P(None, "tp"),
            P(None, "tp"),
            P(None, ("fs", "tp")),
            P(None, ("fs", "tp")),
            P(None, ("fs", "tp")),
            P(("fs", "tp"), None, None),
            P(("fs", "tp"), None, None),
            P(("fs", "tp")),
            P(SP, ("fs", "tp")),
            P(("fs", "tp")),
            P(("fs", "tp")),
            P(),
            P(("fs", "tp"), None),
            P(("fs", "tp"), None),
        ),
        out_specs=P(SP_FS_TP, None),
        check_vma=False,
    )
```

time: 233 us -> 96.3 us (0.41)
  the two profiles are of different devices: /device:TPU:448 before, /device:TPU:64 now
where the time goes in v1:
time: 96.3 us; the launch traced here: 96 us
  Pallas kernels  93.2 us (97%)
  local copies, waits for them, and re-layouts  2.14 us (2%)
    pallas_call x1, Pallas kernels, mix_call(): pl.pallas_call(mix_kernel, out_shape=[jax.ShapeDtypeStruct((8, rows, 128)...  55.5 us
    pallas_call x1, Pallas kernels, output_call(): pl.pallas_call(output_kernel, out_shape=jax.ShapeDtypeStruct((rows // 8,...  23.3 us
    pallas_call x1, Pallas kernels, project_call(): pl.pallas_call(functools.partial(project_kernel, q_scale), out_shape=[jax...  14.4 us

profile of v1, /device:TPU:64, one launch (start us, length us, event | category | flops | bytes accessed | tf_op | source)
XLA Modules:
  0.0 96.0 jit_solution(6483593828567699753)
XLA Ops:
  0.0 14.4 %project.1 = (bf16[256,128]{1,0:T(8,128)(2,1)}, bf16[256,256]{1,0:T(8,128)(2,1)}, bf16[256,128]{1,0:T(8,128)(2,1)}, bf16[256,128]{1,0:T(8,128)(2,1)}) custom-call(bf16[32,2048]{1,0:T(8,128)(2,1)} %tok.1, f32[1,2048]{1,0:T(1,128)} %bitcast.6, bf16[2048,128]{1,0:T(8,128)(2,1)} %wq.1, bf16[2048,128]{1,0:T(8,128)(2,1)} %wk.1, bf16[2048,128]{1,0:T(8,128)(2,1)} %wv.1, ...), custom_call_target="tpu_custom_call" | custom-call | tf_op jit(solution)/shard_map/project/pallas_call | solution.py:136
  14.4 55.5 %mix.1 = (bf16[8,256,128]{2,1,0:T(8,128)(2,1)}, f32[8,256]{1,0:T(8,128)}, bf16[256,128]{1,0:T(8,128)(2,1)}) custom-call(bf16[256,128]{1,0:T(8,128)(2,1)} %get-tuple-element.12.q_ref, bf16[256,256]{1,0:T(8,128)(2,1)} %get-tuple-element.13.kv_ref, bf16[256,128]{1,0:T(8,128)(2,1)} %get-tuple-element.14.lru_in, bf16[256,128]{1,0:T(8,128)(2,1)} %get-tuple-element.15.gate, ...), custom_call_target="tpu_custom_call" | custom-call | tf_op jit(solution)/shard_map/mix/pallas_call | solution.py:459
  70.6 0.6 broadcast_in_dim.8.lam
  71.2 23.3 %output.1 = bf16[32,2048]{1,0:T(8,128)(2,1)} custom-call(bf16[8,256,128]{2,1,0:T(8,128)(2,1)} %get-tuple-element.16.o_ref, f32[8,256]{1,0:T(8,128)} %get-tuple-element.17.lse_ref, bf16[256,128]{1,0:T(8,128)(2,1)} %get-tuple-element.18.lru, f32[1,128]{1,0:T(1,128)} %broadcast_in_dim.8.lam, f32[1,128]{1,0:T(1,128)} %bitcast.7, bf16[128,2048]{1,0:T(8,128)(2,1)} %w_lru.1, ...), custom_call_target="tpu_custom_call" | custom-call | tf_op jit(solution)/shard_map/output/pallas_call | solution.py:602
  94.5 1.6 %copy.20 = bf16[32,2048]{1,0:T(8,128)(2,1)} copy(bf16[32,2048]{1,0:T(8,128)(2,1)} %output.1) | data formatting | bytes 262144
